TPU v7x, 32 devices: a whole 2x2x4 slice. The times are simulated.
32 devices in a mesh: ep: 16 (over z, y, x), tp: 2 (over core).
Axes of the slice: x: 2, y: 2, z: 4, core: 2. Of those that a mesh axis runs over, the one named last changes fastest.
Arguments:
- tokens: bfloat16 [384, 2048], P('ep'), may hold values from -6 to 6
- attn_gain: float32 [2048], replicated, may hold values from 0.1 to 1.9
- w_query: bfloat16 [2048, 1024], P(None, 'tp'), may hold values from -0.125 to 0.125
- w_key: bfloat16 [2048, 1024], P(None, 'tp'), may hold values from -0.125 to 0.125
- w_value: bfloat16 [2048, 1024], P(None, 'tp'), may hold values from -0.125 to 0.125
- w_zgate: bfloat16 [2048, 1024], P(None, 'tp'), may hold values from -0.125 to 0.125
- w_decay: bfloat16 [2048, 8], P(None, 'tp'), may hold values from -0.125 to 0.125
- w_beta: bfloat16 [2048, 8], P(None, 'tp'), may hold values from -0.125 to 0.125
- decay_rate: float32 [8], P('tp'), may hold values from 0.05 to 2
- decay_bias: float32 [8], P('tp'), may hold values from -3 to 3
- state: float32 [384, 8, 128, 128], P('ep', 'tp'), may hold values from -2 to 2
- out_gain: float32 [128], replicated, may hold values from 0.1 to 1.9
- w_out: bfloat16 [1024, 2048], P('tp'), may hold values from -0.1875 to 0.1875
- ffn_gain: float32 [2048], replicated, may hold values from 0.1 to 1.9
- expert_gate: bfloat16 [16, 2048, 512], P('ep', None, 'tp'), may hold values from -0.125 to 0.125
- expert_up: bfloat16 [16, 2048, 512], P('ep', None, 'tp'), may hold values from -0.125 to 0.125
- expert_down: bfloat16 [16, 512, 2048], P('ep', 'tp'), may hold values from -0.25 to 0.25
- routes: int32 [384, 2], P('ep'), may hold values from 0 to 15, all different within a row; in each aligned block of 24 rows (0 to 23, 24 to 47, ...) at most 6 rows name the same one
- route_weight: float32 [384, 2], P('ep'), may hold values from 0.2 to 1
Outputs:
- layer_out: bfloat16 [384, 2048], P('ep', 'tp')
- new_state: float32 [384, 8, 128, 128], P('ep', 'tp')
Inputs may be any that keep to these rules, and one draw needn't show every extreme that they name: `routes`: the 2 entries of a row differ. Among the rows of one index of ep (aligned blocks of 24 rows) no expert is named more than 6 times, a bound that some block reaches.
All inputs are finite; a program needn't handle non-finite values.
Results may differ from a plain program's by a relative error of at most 0.014.
Values may be sent and summed in bfloat16 or wider, within the bound.
A program may use at most 128 MiB of HBM per device.

v0:
```python
import jax
import jax.numpy as jnp
from jax import lax
from jax.sharding import PartitionSpec as P

EPS = 1e-06


def rms_scale(rows, gain):
    return rows * lax.rsqrt(jnp.mean(rows * rows, axis=-1, keepdims=True) + EPS) * gain


def unit_rows(rows):
    return rows * lax.rsqrt(jnp.sum(rows * rows, axis=-1, keepdims=True) + EPS)


def per_device(
    tokens,
    attn_gain,
    w_query,
    w_key,
    w_value,
    w_zgate,
    w_decay,
    w_beta,
    decay_rate,
    decay_bias,
    state,
    out_gain,
    w_out,
    ffn_gain,
    expert_gate,
    expert_up,
    expert_down,
    routes,
    route_weight,
):
    seqs, width = tokens.shape
    heads = state.shape[1]
    head_dim = state.shape[2]
    top = routes.shape[1]
    resid_in = tokens.astype(jnp.float32)
    normed = rms_scale(resid_in, attn_gain).astype(jnp.bfloat16)

    def project(weight):
        return jnp.dot(normed, weight, preferred_element_type=jnp.float32).astype(jnp.bfloat16)

    def heads_of(raw):
        return raw.reshape(seqs, heads, head_dim).astype(jnp.float32)

    query = unit_rows(jax.nn.silu(heads_of(project(w_query)))) * head_dim ** (-0.5)
    key = unit_rows(jax.nn.silu(heads_of(project(w_key))))
    value = jax.nn.silu(heads_of(project(w_value)))
    zmul = jax.nn.silu(heads_of(project(w_zgate)))
    fade = jnp.exp(-decay_rate * jax.nn.softplus(project(w_decay).astype(jnp.float32) + decay_bias))
    beta = jax.nn.sigmoid(project(w_beta).astype(jnp.float32))
    predicted = jnp.einsum("shkv,shk->shv", state, key, precision=lax.Precision.HIGHEST)
    written = beta[..., None] * (value - fade[..., None] * predicted)
    new_state = fade[..., None, None] * state + key[..., :, None] * written[..., None, :]
    read = jnp.einsum("shkv,shk->shv", new_state, query, precision=lax.Precision.HIGHEST)
    heads_out = (
        (rms_scale(read, out_gain) * zmul).astype(jnp.bfloat16).reshape(seqs, heads * head_dim)
    )
    partial_value = jnp.dot(heads_out, w_out, preferred_element_type=jnp.float32)
    mixed = lax.psum(partial_value.astype(jnp.bfloat16), "tp").astype(jnp.float32)
    resid = resid_in + mixed
    moe_in = rms_scale(resid, ffn_gain).astype(jnp.bfloat16)
    experts = lax.axis_size("ep")
    cap = max(2, 2 * seqs * top // experts)
    flat_routes = routes.reshape(-1)
    onehot = (flat_routes[:, None] == jnp.arange(experts, dtype=jnp.int32)[None, :]).astype(
        jnp.int32
    )
    before = jnp.cumsum(onehot, axis=0) - onehot
    slot = jnp.sum(before * onehot, axis=1)
    place = flat_routes * cap + slot
    pick = (place[:, None] == jnp.arange(experts * cap, dtype=jnp.int32)[None, :]).astype(
        jnp.bfloat16
    )
    columns = width // lax.axis_size("tp")
    own_part = lax.dynamic_slice_in_dim(moe_in, lax.axis_index("tp") * columns, columns, 1)
    spread = jnp.repeat(own_part, top, axis=0)
    outgoing = jnp.dot(pick.T, spread, preferred_element_type=jnp.float32).astype(jnp.bfloat16)
    outgoing = outgoing.reshape(experts, 1, cap, columns)
    arrived = lax.all_gather(
        lax.all_to_all(outgoing, "ep", split_axis=0, concat_axis=1, tiled=True),
        "tp",
        axis=3,
        tiled=True,
    )
    flat_rows = arrived.reshape(-1, arrived.shape[-1])
    gate = jnp.dot(flat_rows, expert_gate[0], preferred_element_type=jnp.float32)
    up = jnp.dot(flat_rows, expert_up[0], preferred_element_type=jnp.float32)
    hidden = (jax.nn.silu(gate) * up).astype(jnp.bfloat16)
    term = jnp.dot(hidden, expert_down[0], preferred_element_type=jnp.float32)
    terms = term.reshape(arrived.shape[:-1] + (term.shape[-1],))
    summed = lax.psum_scatter(terms.astype(jnp.bfloat16), "tp", scatter_dimension=3, tiled=True)
    returned = lax.all_to_all(summed, "ep", split_axis=1, concat_axis=0, tiled=True)
    returned = returned.reshape(experts * cap, columns)
    per_route = jnp.dot(pick, returned, preferred_element_type=jnp.float32).reshape(
        seqs, top, columns
    )
    combined = jnp.sum(per_route * route_weight[..., None], axis=1)
    own_resid = lax.dynamic_slice_in_dim(resid, lax.axis_index("tp") * columns, columns, 1)
    layer_out = (own_resid + combined).astype(jnp.bfloat16)
    return (layer_out, new_state)


def solution(mesh):
    in_specs = (
        P("ep", None),
        P(),
        P(None, "tp"),
        P(None, "tp"),
        P(None, "tp"),
        P(None, "tp"),
        P(None, "tp"),
        P(None, "tp"),
        P("tp"),
        P("tp"),
        P("ep", "tp", None, None),
        P(),
        P("tp", None),
        P(),
        P("ep", None, "tp"),
        P("ep", None, "tp"),
        P("ep", "tp", None),
        P("ep", None),
        P("ep", None),
    )
    out_specs = (P("ep", "tp"), P("ep", "tp", None, None))
    return jax.shard_map(
        per_device, mesh=mesh, in_specs=in_specs, out_specs=out_specs, check_vma=False
    )
```

profile of v0, /device:TPU:0, one launch (start us, length us, event | category | flops | bytes accessed | tf_op | source)
XLA Modules:
  0.0 115.3 jit_solution(10898759450930380615)
XLA Ops:
  7.2 0.0 copy-start
  7.2 0.0 copy-start.2
  7.2 0.0 copy-start.5
  7.2 0.0 copy-start.12
  7.2 0.0 all-reduce.2.cloned.1.call-start
  7.3 1.2 %fusion.18 = f32[24]{0:T(128)S(1)} fusion(bf16[24,2048]{1,0:T(8,128)(2,1)} %param.19), kind=kLoop, calls=%fused_computation.33 | loop fusion | flops 147432 | bytes 98400 | tf_op jit(solution)/shard_map/reduce_sum | solution.py:10
  8.4 0.0 copy-start.11
  8.5 2.1 %fusion.6 = f32[24,512]{1,0:T(8,128)S(1)} fusion(bf16[2048,512]{1,0:T(8,128)(2,1)} %param.22, bf16[24,2048]{1,0:T(8,128)(2,1)} %param.19, f32[2048]{0:T(1024)} %param.20, f32[24]{0:T(128)S(1)} %add_rsqrt_fusion.4), kind=kOutput, calls=%fused_computation.16 | convolution fusion | flops 50552832 | bytes 2252896 | tf_op jit(solution)/shard_map/dot_general | solution.py:46
  10.6 0.1 multiply_reduce_fusion.3
  10.7 0.1 broadcast_multiply_fusion
  10.8 0.0 copy-done.12
  10.9 0.2 fusion.34
  11.1 0.1 copy.48
  11.2 2.0 %fusion.5 = f32[24,512]{1,0:T(8,128)S(1)} fusion(bf16[2048,512]{1,0:T(8,128)(2,1)} %param.23, bf16[24,2048]{1,0:T(8,128)(2,1)S(1)} %copy-done.2, f32[2048]{0:T(1024)S(1)} %copy-done.5, f32[24]{0:T(128)S(1)} %add_rsqrt_fusion.4), kind=kOutput, calls=%fused_computation.14 | convolution fusion | flops 50552832 | bytes 2252896 | tf_op jit(solution)/shard_map/dot_general | solution.py:46
  13.3 0.2 fusion.13
  13.5 0.1 copy.49
  13.6 8.1 %fusion.41 = f32[24,4,1,128]{3,2,1,0:T(1,128)S(1)} fusion(f32[24,4,128,1]{2,3,1,0:T(1,128)S(1)} %bitcast.48, f32[24,4,128,128]{3,2,1,0:T(8,128)} %param.29), kind=kOutput, calls=%fused_computation.73 | convolution fusion | flops 18874368 | bytes 6389760 | tf_op jit(solution)/shard_map/shkv,shk->shv/dot_general | solution.py:57
  21.7 0.1 fusion.24
  21.8 0.0 copy-start.3
  21.8 3.9 %multiply_add_fusion = f32[24,4,128,128]{3,2,1,0:T(8,128)} fusion(f32[24,4,128,128]{3,2,1,0:T(8,128)S(1)} %copy-done.1, f32[24,4,128]{2,1,0:T(4,128)S(1)} %fusion.24, f32[24,4,128]{2,1,0:T(4,128)S(1)} %broadcast_multiply_fusion, f32[24,4]{1,0:T(8,128)S(1)} %copy.48), kind=kLoop, calls=%fused_computation | loop fusion | flops 4718592 | bytes 12681600 | tf_op jit(solution)/shard_map/add | solution.py:59
  25.7 0.4 fusion.4
  26.2 0.1 multiply_reduce_fusion.2
  26.3 0.1 multiply_multiply_fusion
  26.4 0.0 copy-start.4
  26.4 7.5 %fusion.42 = f32[24,4,1,128]{3,2,1,0:T(1,128)S(1)} fusion(f32[24,4,128,128]{3,2,1,0:T(8,128)} %multiply_add_fusion, f32[24,4,128,1]{2,3,1,0:T(1,128)S(1)} %bitcast.51), kind=kOutput, calls=%fused_computation.74 | convolution fusion | flops 18874368 | bytes 6389760 | tf_op jit(solution)/shard_map/shkv,shk->shv/dot_general | solution.py:60
  33.9 0.1 multiply_reduce_fusion.1
  34.1 0.0 copy-start.6
  34.1 0.0 copy-start.7
  34.1 0.4 fusion.3
  34.6 0.0 copy-done.9
  34.6 0.1 fusion.25
  34.7 1.0 convolution_convert_fusion.1
  35.7 0.0 all-reduce.2.cloned.1.call-update
  35.8 0.0 reduce-scatter.2.cloned.1.call-start
  35.8 0.1 copy.51
  35.9 0.1 eq.50
  36.0 0.1 fusion.28
  36.1 0.1 reduce_window_sum.11
  36.2 0.2 select_reduce_fusion
  36.4 0.0 copy-done.7
  36.4 20.1 %all-reduce.2.cloned.1.call-done = bf16[24,2048]{1,0:T(8,128)(2,1)} async-done(((bf16[24,2048]{1,0:T(8,128)(2,1)}), bf16[24,2048]{1,0:T(8,128)(2,1)}) %all-reduce.2.cloned.1.call-update) | async-done | bytes 98320 | tf_op jit(solution)/shard_map/psum | solution.py:65
  56.5 1.0 multiply_reduce_fusion
  57.5 0.1 multiply_convert_fusion
  57.6 0.1 broadcast_in_dim.2
  57.7 0.3 convolution_convert_fusion.2
  58.0 0.1 reshape.136
  58.1 16.9 %all_to_all.21 = bf16[16,1,6,1024]{3,2,1,0:T(8,128)(2,1)S(1)} all-to-all(bf16[16,1,6,1024]{3,2,1,0:T(8,128)(2,1)S(1)} %bitcast.47), channel_id=1, replica_groups=mesh['ep'=16,'tp'=2] {'ep'}, dimensions={0} | all-to-all | bytes 393216 | tf_op jit(solution)/shard_map/all_to_all | solution.py:86
  75.0 2.2 %all-gather = bf16[16,1,6,2048]{3,2,1,0:T(8,128)(2,1)S(1)} all-gather(bf16[16,1,6,1024]{3,2,1,0:T(8,128)(2,1)S(1)} %all_to_all.21), channel_id=2, replica_groups=mesh['ep'=16,'tp'=2] {'tp'}, dimensions={3}, use_global_device_ids=true | all-gather | bytes 589824 | tf_op jit(solution)/shard_map/all_gather | solution.py:85
  77.2 0.1 reshape.137
  77.3 1.5 %fusion.16 = f32[96,256]{1,0:T(8,128)S(1)} fusion(bf16[96,2048]{1,0:T(8,128)(2,1)S(1)} %reshape.137, bf16[1,2048,256]{2,1,0:T(8,128)(2,1)} %param.33), kind=kOutput, calls=%fused_computation.28 | convolution fusion | flops 100663296 | bytes 1540096 | tf_op jit(solution)/shard_map/dot_general | solution.py:92
  78.9 1.5 %fusion.2 = bf16[96,256]{1,0:T(8,128)(2,1)S(1)} fusion(bf16[96,2048]{1,0:T(8,128)(2,1)S(1)} %reshape.137, bf16[1,2048,256]{2,1,0:T(8,128)(2,1)} %param.34, f32[96,256]{1,0:T(8,128)S(1)} %fusion.16), kind=kOutput, calls=%fused_computation.8 | convolution fusion | flops 100810752 | bytes 1589248 | tf_op jit(solution)/shard_map/dot_general | solution.py:93
  80.4 0.0 copy-start.8
  80.5 2.3 %fusion = bf16[1,16,6,2048]{3,1,2,0:T(8,128)(2,1)} fusion(bf16[1,256,2048]{2,1,0:T(8,128)(2,1)} %param.35, bf16[16,6,256]{2,1,0:T(8,128)(2,1)S(1)} %dot_general.56), kind=kOutput, calls=%fused_computation.2 | convolution fusion | flops 100859904 | bytes 1490944 | tf_op jit(solution)/shard_map/dot_general | solution.py:95
  82.7 0.0 reduce-scatter.2.cloned.1.call-update
  82.8 5.9 %reduce-scatter.2.cloned.1.call-done = bf16[1,16,6,1024]{3,1,2,0:T(8,128)(2,1)} async-done(((bf16[1,16,6,2048]{3,1,2,0:T(8,128)(2,1)}), bf16[1,16,6,1024]{3,1,2,0:T(8,128)(2,1)}) %reduce-scatter.2.cloned.1.call-update) | async-done | bytes 196624 | tf_op jit(solution)/shard_map/reduce_scatter | solution.py:97
  88.6 1.7 %copy.55 = bf16[1,16,6,1024]{3,2,0,1:T(8,128)(2,1)} copy(bf16[1,16,6,1024]{3,1,2,0:T(8,128)(2,1)} %reduce-scatter.2.cloned.1.call-done) | data formatting | bytes 393216 | tf_op jit(solution)/shard_map/reduce_scatter | solution.py:97
  90.4 6.7 %all-to-all-start.1 = ((bf16[1,16,6,1024]{3,2,0,1:T(8,128)(2,1)}), bf16[1,16,6,1024]{3,2,0,1:T(8,128)(2,1)S(1)}, u32[]{:S(2)}, u32[]{:S(2)}) async-start(bf16[1,16,6,1024]{3,2,0,1:T(8,128)(2,1)} %copy.55), calls=%async_computation.2 | async-start | bytes 524288 | tf_op jit(solution)/shard_map/all_to_all | solution.py:98
  97.1 0.1 reduce_sum.70
  97.2 0.1 copy.52
  97.3 10.2 %all-to-all-done.1 = bf16[1,16,6,1024]{3,2,0,1:T(8,128)(2,1)S(1)} async-done(((bf16[1,16,6,1024]{3,2,0,1:T(8,128)(2,1)}), bf16[1,16,6,1024]{3,2,0,1:T(8,128)(2,1)S(1)}, u32[]{:S(2)}, u32[]{:S(2)}) %all-to-all-start.1) | async-done | bytes 196640 | tf_op jit(solution)/shard_map/all_to_all | solution.py:98
  107.5 0.1 reshape.150
  107.6 0.0 copy-done.8
  107.6 0.2 fusion.1
  107.8 0.6 add_convert_fusion
  (29 shorter events, 0.2 us)
Async XLA Ops:
  7.2 27.5 %copy-start = (bf16[512,2048]{1,0:T(8,128)(2,1)S(1)}, bf16[512,2048]{1,0:T(8,128)(2,1)}, u32[]{:S(2)}) copy-start(bf16[512,2048]{1,0:T(8,128)(2,1)} %param.31) | copy-start | bytes 6291460
  7.2 3.7 %copy-start.2 = (bf16[24,2048]{1,0:T(8,128)(2,1)S(1)}, bf16[24,2048]{1,0:T(8,128)(2,1)}, u32[]{:S(2)}) copy-start(bf16[24,2048]{1,0:T(8,128)(2,1)} %param.19) | copy-start | bytes 294916
  7.2 3.7 %copy-start.5 = (f32[2048]{0:T(1024)S(1)}, f32[2048]{0:T(1024)}, u32[]{:S(2)}) copy-start(f32[2048]{0:T(1024)} %param.20) | copy-start | bytes 24580
  7.2 3.6 %copy-start.12 = (f32[4]{0:T(128)S(1)}, f32[4]{0:T(128)}, u32[]{:S(2)}) copy-start(f32[4]{0:T(128)} %param.27) | copy-start | bytes 52
  7.2 3.7 %copy-start.10 = (bf16[2048,4]{0,1:T(4,128)(2,1)S(1)}, bf16[2048,4]{0,1:T(4,128)(2,1)}, u32[]{:S(2)}) copy-start(bf16[2048,4]{0,1:T(4,128)(2,1)} %param.25) | copy-start | bytes 49156
  7.2 3.7 %copy-start.13 = (f32[4]{0:T(128)S(1)}, f32[4]{0:T(128)}, u32[]{:S(2)}) copy-start(f32[4]{0:T(128)} %param.28) | copy-start | bytes 52
  7.2 49.2 %all-reduce.2.cloned.1.call-start = ((), (), s32[]{:S(2)}) async-start(), calls=%async_computation.3 | async-start | bytes 196608 | tf_op jit(solution)/shard_map/psum | solution.py:65
  8.4 4.8 %copy-start.11 = (bf16[2048,4]{0,1:T(4,128)(2,1)S(1)}, bf16[2048,4]{0,1:T(4,128)(2,1)}, u32[]{:S(2)}) copy-start(bf16[2048,4]{0,1:T(4,128)(2,1)} %param.26) | copy-start | bytes 49156
  13.6 8.2 %copy-start.1 = (f32[24,4,128,128]{3,2,1,0:T(8,128)S(1)}, f32[24,4,128,128]{3,2,1,0:T(8,128)}, u32[]{:S(2)}) copy-start(f32[24,4,128,128]{3,2,1,0:T(8,128)} %param.29) | copy-start | bytes 18874372
  21.8 3.9 %copy-start.3 = (bf16[2048,512]{1,0:T(8,128)(2,1)S(1)}, bf16[2048,512]{1,0:T(8,128)(2,1)}, u32[]{:S(2)}) copy-start(bf16[2048,512]{1,0:T(8,128)(2,1)} %param.21) | copy-start | bytes 6291460
  26.4 7.7 %copy-start.4 = (bf16[2048,512]{1,0:T(8,128)(2,1)S(1)}, bf16[2048,512]{1,0:T(8,128)(2,1)}, u32[]{:S(2)}) copy-start(bf16[2048,512]{1,0:T(8,128)(2,1)} %param.24) | copy-start | bytes 6291460
  33.9 0.7 copy-start.9
  34.1 1.7 %copy-start.6 = (s32[24,2]{0,1:T(2,128)S(1)}, s32[24,2]{0,1:T(2,128)}, u32[]{:S(2)}) copy-start(s32[24,2]{0,1:T(2,128)} %param.36) | copy-start | bytes 580
  34.1 2.3 %copy-start.7 = (f32[2048]{0:T(1024)S(1)}, f32[2048]{0:T(1024)}, u32[]{:S(2)}) copy-start(f32[2048]{0:T(1024)} %param.32) | copy-start | bytes 24580
  35.8 52.9 %reduce-scatter.2.cloned.1.call-start = ((), (), s32[]{:S(2)}) async-start(), calls=%async_computation.4 | async-start | bytes 589824 | tf_op jit(solution)/shard_map/reduce_scatter | solution.py:97
  80.4 27.2 %copy-start.8 = (f32[24,2]{0,1:T(2,128)S(1)}, f32[24,2]{0,1:T(2,128)}, u32[]{:S(2)}) copy-start(f32[24,2]{0,1:T(2,128)} %param.37) | copy-start | bytes 580
  90.4 17.1 %all-to-all-start.1 = ((bf16[1,16,6,1024]{3,2,0,1:T(8,128)(2,1)}), bf16[1,16,6,1024]{3,2,0,1:T(8,128)(2,1)S(1)}, u32[]{:S(2)}, u32[]{:S(2)}) async-start(bf16[1,16,6,1024]{3,2,0,1:T(8,128)(2,1)} %copy.55), calls=%async_computation.2 | async-start | bytes 524288 | tf_op jit(solution)/shard_map/all_to_all | solution.py:98
Sparse Core Ops, SparseCore 0:
  35.9 20.5 all-reduce.1
  82.9 5.7 reduce-scatter.1
where the time goes:
time: 116 us; the launch traced here: 115 us
  waiting for transfers between devices  36.2 us (31%)
  matrix products  28 us (24%)
  blocking collectives  19.1 us (16%)
  between operations  14.4 us (12%)
  other arithmetic  7.91 us (7%)
  starting transfers between devices  6.81 us (6%)
  local copies, waits for them, and re-layouts  2.86 us (2%)
    psum x1, waiting for transfers between devices, per_device(): lax.psum(partial_value.astype(jnp.bfloat16), 'tp').astype(jnp.float32)  20.1 us
    all_to_all x1, blocking collectives, per_device(): lax.all_to_all(outgoing, 'ep', split_axis=0, concat_axis=1, tiled=True)  16.9 us
    all_to_all x1, waiting for transfers between devices, per_device(): lax.all_to_all(summed, 'ep', split_axis=1, concat_axis=0, tiled=True)  10.2 us
    dot_general x1, matrix products, per_device(): jnp.einsum('shkv,shk->shv', state, key, precision=lax.Precision.HIGHEST)  8.09 us
    dot_general x1, matrix products, per_device(): jnp.einsum('shkv,shk->shv', new_state, query, precision=lax.Precision.HIG...  7.54 us
    all_to_all x1, starting transfers between devices, per_device(): lax.all_to_all(summed, 'ep', split_axis=1, concat_axis=0, tiled=True)  6.73 us
    reduce_scatter x1, waiting for transfers between devices, per_device(): lax.psum_scatter(terms.astype(jnp.bfloat16), 'tp', scatter_dimension=3, t...  5.89 us
    dot_general x6, matrix products, project(): jnp.dot(normed, weight, preferred_element_type=jnp.float32)  5.45 us
  transfers between devices with their start and end apart: 3, of which 3 were waited for; matrix products, arithmetic and copies ran while one was open for 1% of the time, Pallas kernels for 0%

commit v1 on v0

--- a/solution.py
+++ b/solution.py
@@ -1,9 +1,19 @@
+import functools
 import jax
 import jax.numpy as jnp
 from jax import lax
 from jax.sharding import PartitionSpec as P
 
 EPS = 1e-06
+
+
+def name_area(slab_in, mesh_name):
+    built = lax.all_gather(slab_in, mesh_name)
+    k_now = jnp.sum(built, 0)
+    return k_now
+
+
+move_types = functools.partial(name_area, mesh_name="tp")
 
 
 def rms_scale(rows, gain):
@@ -62,7 +72,7 @@
         (rms_scale(read, out_gain) * zmul).astype(jnp.bfloat16).reshape(seqs, heads * head_dim)
     )
     partial_value = jnp.dot(heads_out, w_out, preferred_element_type=jnp.float32)
-    mixed = lax.psum(partial_value.astype(jnp.bfloat16), "tp").astype(jnp.float32)
+    mixed = move_types(partial_value.astype(jnp.bfloat16)).astype(jnp.float32)
     resid = resid_in + mixed
     moe_in = rms_scale(resid, ffn_gain).astype(jnp.bfloat16)
     experts = lax.axis_size("ep")

time: 116 us -> 97.5 us (0.84)
  waiting for transfers between devices: 36.2 us -> 16.1 us
  blocking collectives: 19.1 us -> 22.4 us
    psum x1 -> x0, waiting for transfers between devices: 20.1 us -> none  [per_device(): lax.psum(partial_value.astype(jnp.bfloat16), 'tp').astype(jnp.float32)]
    all_gather x0 -> x1, blocking collectives: none -> 2.08 us  [name_area(): built = lax.all_gather(slab_in, mesh_name)]
    all_to_all x1, blocking collectives: 16.9 us -> 18.2 us  [per_device(): lax.all_to_all(outgoing, 'ep', split_axis=0, concat_axis=1, tiled=True)]
  transfers between devices with their start and end apart: 3 -> 2, of which waited for: 3 -> 2; matrix products, arithmetic and copies ran while one was open for 1% -> 0% of each run, Pallas kernels for 0% -> 0%
where the time goes in v1:
time: 97.5 us; the launch traced here: 97 us
  matrix products  27.3 us (28%)
  blocking collectives  22.4 us (23%)
  waiting for transfers between devices  16.1 us (17%)
  between operations  14.4 us (15%)
  other arithmetic  7.05 us (7%)
  starting transfers between devices  6.77 us (7%)
  local copies, waits for them, and re-layouts  2.87 us (3%)
    all_to_all x1, blocking collectives, per_device(): lax.all_to_all(outgoing, 'ep', split_axis=0, concat_axis=1, tiled=True)  18.2 us
    all_to_all x1, waiting for transfers between devices, per_device(): lax.all_to_all(summed, 'ep', split_axis=1, concat_axis=0, tiled=True)  10.2 us
    dot_general x1, matrix products, per_device(): jnp.einsum('shkv,shk->shv', state, key, precision=lax.Precision.HIGHEST)  8.09 us
    dot_general x1, matrix products, per_device(): jnp.einsum('shkv,shk->shv', new_state, query, precision=lax.Precision.HIG...  7.54 us
    all_to_all x1, starting transfers between devices, per_device(): lax.all_to_all(summed, 'ep', split_axis=1, concat_axis=0, tiled=True)  6.73 us
    reduce_scatter x1, waiting for transfers between devices, per_device(): lax.psum_scatter(terms.astype(jnp.bfloat16), 'tp', scatter_dimension=3, t...  5.89 us
    dot_general x6, matrix products, project(): jnp.dot(normed, weight, preferred_element_type=jnp.float32)  5.45 us
    add x1, other arithmetic, per_device(): fade[..., None, None] * state + key[..., :, None] * written[..., None, :]  3.86 us
  transfers between devices with their start and end apart: 2, of which 2 were waited for; matrix products, arithmetic and copies ran while one was open for 0% of the time, Pallas kernels for 0%

profile of v1, /device:TPU:0, one launch (start us, length us, event | category | flops | bytes accessed | tf_op | source)
XLA Modules:
  0.0 97.0 jit_solution(6332632693819059333)
XLA Ops:
  7.2 0.0 copy-start
  7.2 0.0 copy-start.2
  7.2 0.0 copy-start.5
  7.2 0.0 copy-start.12
  7.2 0.0 copy-start.10
  7.2 0.0 copy-start.13
  7.2 0.0 reduce-scatter.2.cloned.1.call-start
  7.3 1.2 %fusion.18 = f32[24]{0:T(128)S(1)} fusion(bf16[24,2048]{1,0:T(8,128)(2,1)} %param.19), kind=kLoop, calls=%fused_computation.33 | loop fusion | flops 147432 | bytes 98400 | tf_op jit(solution)/shard_map/reduce_sum | solution.py:20
  8.4 0.0 copy-start.11
  8.5 2.1 %fusion.6 = f32[24,512]{1,0:T(8,128)S(1)} fusion(bf16[2048,512]{1,0:T(8,128)(2,1)} %param.22, bf16[24,2048]{1,0:T(8,128)(2,1)} %param.19, f32[2048]{0:T(1024)} %param.20, f32[24]{0:T(128)S(1)} %add_rsqrt_fusion.4), kind=kOutput, calls=%fused_computation.16 | convolution fusion | flops 50552832 | bytes 2252896 | tf_op jit(solution)/shard_map/dot_general | solution.py:56
  10.6 0.1 multiply_reduce_fusion.3
  10.7 0.1 broadcast_multiply_fusion
  10.9 0.2 fusion.34
  11.1 0.1 copy.48
  11.2 2.0 %fusion.5 = f32[24,512]{1,0:T(8,128)S(1)} fusion(bf16[2048,512]{1,0:T(8,128)(2,1)} %param.23, bf16[24,2048]{1,0:T(8,128)(2,1)S(1)} %copy-done.2, f32[2048]{0:T(1024)S(1)} %copy-done.5, f32[24]{0:T(128)S(1)} %add_rsqrt_fusion.4), kind=kOutput, calls=%fused_computation.14 | convolution fusion | flops 50552832 | bytes 2252896 | tf_op jit(solution)/shard_map/dot_general | solution.py:56
  13.3 0.0 copy-done.11
  13.3 0.2 fusion.13
  13.5 0.1 copy.49
  13.6 8.1 %fusion.41 = f32[24,4,1,128]{3,2,1,0:T(1,128)S(1)} fusion(f32[24,4,128,1]{2,3,1,0:T(1,128)S(1)} %bitcast.50, f32[24,4,128,128]{3,2,1,0:T(8,128)} %param.29), kind=kOutput, calls=%fused_computation.73 | convolution fusion | flops 18874368 | bytes 6389760 | tf_op jit(solution)/shard_map/shkv,shk->shv/dot_general | solution.py:67
  21.7 0.1 fusion.24
  21.8 0.0 copy-done.1
  21.8 0.0 copy-start.3
  21.8 3.9 %multiply_add_fusion = f32[24,4,128,128]{3,2,1,0:T(8,128)} fusion(f32[24,4,128,128]{3,2,1,0:T(8,128)S(1)} %copy-done.1, f32[24,4,128]{2,1,0:T(4,128)S(1)} %fusion.24, f32[24,4,128]{2,1,0:T(4,128)S(1)} %broadcast_multiply_fusion, f32[24,4]{1,0:T(8,128)S(1)} %copy.48), kind=kLoop, calls=%fused_computation | loop fusion | flops 4718592 | bytes 12681600 | tf_op jit(solution)/shard_map/add | solution.py:69
  25.7 0.0 copy-done.3
  25.7 0.4 fusion.4
  26.2 0.1 multiply_reduce_fusion.2
  26.3 0.1 multiply_multiply_fusion
  26.4 0.0 copy-start.4
  26.4 7.5 %fusion.42 = f32[24,4,1,128]{3,2,1,0:T(1,128)S(1)} fusion(f32[24,4,128,128]{3,2,1,0:T(8,128)} %multiply_add_fusion, f32[24,4,128,1]{2,3,1,0:T(1,128)S(1)} %bitcast.53), kind=kOutput, calls=%fused_computation.74 | convolution fusion | flops 18874368 | bytes 6389760 | tf_op jit(solution)/shard_map/shkv,shk->shv/dot_general | solution.py:70
  33.9 0.1 multiply_reduce_fusion.1
  34.1 0.4 fusion.3
  34.5 0.1 copy-done.9
  34.6 0.1 fusion.25
  34.7 0.0 copy-done
  34.7 0.4 convolution_convert_fusion.1
  35.1 2.1 %all-gather = bf16[48,2048]{1,0:T(8,128)(2,1)S(1)} all-gather(bf16[24,2048]{1,0:T(8,128)(2,1)S(1)} %convolution_convert_fusion.1), channel_id=2, replica_groups=mesh['ep'=16,'tp'=2] {'tp'}, dimensions={0}, use_global_device_ids=true | all-gather | bytes 294912 | tf_op jit(solution)/shard_map/all_gather | solution.py:11
  37.2 0.1 multiply_reduce_fusion
  37.4 0.1 multiply_convert_fusion
  37.5 0.1 broadcast_in_dim.2
  37.6 0.1 copy.51
  37.7 0.1 eq.50
  37.8 0.1 fusion.28
  37.9 0.1 reduce_window_sum.11
  37.9 0.2 select_reduce_fusion
  38.1 0.3 convolution_convert_fusion.2
  38.5 0.1 reshape.136
  38.6 18.2 %all_to_all.21 = bf16[16,1,6,1024]{3,2,1,0:T(8,128)(2,1)S(1)} all-to-all(bf16[16,1,6,1024]{3,2,1,0:T(8,128)(2,1)S(1)} %bitcast.48), channel_id=1, replica_groups=mesh['ep'=16,'tp'=2] {'ep'}, dimensions={0} | all-to-all | bytes 393216 | tf_op jit(solution)/shard_map/all_to_all | solution.py:96
  56.7 2.2 %all-gather.1 = bf16[16,1,6,2048]{3,2,1,0:T(8,128)(2,1)S(1)} all-gather(bf16[16,1,6,1024]{3,2,1,0:T(8,128)(2,1)S(1)} %all_to_all.21), channel_id=3, replica_groups=mesh['ep'=16,'tp'=2] {'tp'}, dimensions={3}, use_global_device_ids=true | all-gather | bytes 589824 | tf_op jit(solution)/shard_map/all_gather | solution.py:95
  58.9 0.1 reshape.137
  59.1 1.5 %fusion.16 = f32[96,256]{1,0:T(8,128)S(1)} fusion(bf16[96,2048]{1,0:T(8,128)(2,1)S(1)} %reshape.137, bf16[1,2048,256]{2,1,0:T(8,128)(2,1)} %param.33), kind=kOutput, calls=%fused_computation.28 | convolution fusion | flops 100663296 | bytes 1540096 | tf_op jit(solution)/shard_map/dot_general | solution.py:102
  60.6 1.5 %fusion.2 = bf16[96,256]{1,0:T(8,128)(2,1)S(1)} fusion(bf16[96,2048]{1,0:T(8,128)(2,1)S(1)} %reshape.137, bf16[1,2048,256]{2,1,0:T(8,128)(2,1)} %param.34, f32[96,256]{1,0:T(8,128)S(1)} %fusion.16), kind=kOutput, calls=%fused_computation.8 | convolution fusion | flops 100810752 | bytes 1589248 | tf_op jit(solution)/shard_map/dot_general | solution.py:103
  62.1 0.0 copy-start.8
  62.2 2.3 %fusion = bf16[1,16,6,2048]{3,1,2,0:T(8,128)(2,1)} fusion(bf16[1,256,2048]{2,1,0:T(8,128)(2,1)} %param.35, bf16[16,6,256]{2,1,0:T(8,128)(2,1)S(1)} %dot_general.56), kind=kOutput, calls=%fused_computation.2 | convolution fusion | flops 100859904 | bytes 1490944 | tf_op jit(solution)/shard_map/dot_general | solution.py:105
  64.4 0.0 reduce-scatter.2.cloned.1.call-update
  64.5 5.9 %reduce-scatter.2.cloned.1.call-done = bf16[1,16,6,1024]{3,1,2,0:T(8,128)(2,1)} async-done(((bf16[1,16,6,2048]{3,1,2,0:T(8,128)(2,1)}), bf16[1,16,6,1024]{3,1,2,0:T(8,128)(2,1)}) %reduce-scatter.2.cloned.1.call-update) | async-done | bytes 196624 | tf_op jit(solution)/shard_map/reduce_scatter | solution.py:107
  70.4 1.7 %copy.55 = bf16[1,16,6,1024]{3,2,0,1:T(8,128)(2,1)} copy(bf16[1,16,6,1024]{3,1,2,0:T(8,128)(2,1)} %reduce-scatter.2.cloned.1.call-done) | data formatting | bytes 393216 | tf_op jit(solution)/shard_map/reduce_scatter | solution.py:107
  72.1 6.7 %all-to-all-start.1 = ((bf16[1,16,6,1024]{3,2,0,1:T(8,128)(2,1)}), bf16[1,16,6,1024]{3,2,0,1:T(8,128)(2,1)S(1)}, u32[]{:S(2)}, u32[]{:S(2)}) async-start(bf16[1,16,6,1024]{3,2,0,1:T(8,128)(2,1)} %copy.55), calls=%async_computation.2 | async-start | bytes 524288 | tf_op jit(solution)/shard_map/all_to_all | solution.py:108
  78.8 0.1 reduce_sum.83
  78.9 0.1 copy.52
  79.0 10.2 %all-to-all-done.1 = bf16[1,16,6,1024]{3,2,0,1:T(8,128)(2,1)S(1)} async-done(((bf16[1,16,6,1024]{3,2,0,1:T(8,128)(2,1)}), bf16[1,16,6,1024]{3,2,0,1:T(8,128)(2,1)S(1)}, u32[]{:S(2)}, u32[]{:S(2)}) %all-to-all-start.1) | async-done | bytes 196640 | tf_op jit(solution)/shard_map/all_to_all | solution.py:108
  89.2 0.1 reshape.151
  89.3 0.0 copy-done.8
  89.3 0.2 fusion.1
  89.5 0.6 add_convert_fusion
  (28 shorter events, 0.3 us)
Async XLA Ops:
  7.2 27.5 %copy-start = (bf16[512,2048]{1,0:T(8,128)(2,1)S(1)}, bf16[512,2048]{1,0:T(8,128)(2,1)}, u32[]{:S(2)}) copy-start(bf16[512,2048]{1,0:T(8,128)(2,1)} %param.31) | copy-start | bytes 6291460
  7.2 3.7 %copy-start.2 = (bf16[24,2048]{1,0:T(8,128)(2,1)S(1)}, bf16[24,2048]{1,0:T(8,128)(2,1)}, u32[]{:S(2)}) copy-start(bf16[24,2048]{1,0:T(8,128)(2,1)} %param.19) | copy-start | bytes 294916
  7.2 3.7 %copy-start.5 = (f32[2048]{0:T(1024)S(1)}, f32[2048]{0:T(1024)}, u32[]{:S(2)}) copy-start(f32[2048]{0:T(1024)} %param.20) | copy-start | bytes 24580
  7.2 3.6 %copy-start.12 = (f32[4]{0:T(128)S(1)}, f32[4]{0:T(128)}, u32[]{:S(2)}) copy-start(f32[4]{0:T(128)} %param.27) | copy-start | bytes 52
  7.2 3.7 %copy-start.10 = (bf16[2048,4]{0,1:T(4,128)(2,1)S(1)}, bf16[2048,4]{0,1:T(4,128)(2,1)}, u32[]{:S(2)}) copy-start(bf16[2048,4]{0,1:T(4,128)(2,1)} %param.25) | copy-start | bytes 49156
  7.2 3.7 %copy-start.13 = (f32[4]{0:T(128)S(1)}, f32[4]{0:T(128)}, u32[]{:S(2)}) copy-start(f32[4]{0:T(128)} %param.28) | copy-start | bytes 52
  7.2 63.1 %reduce-scatter.2.cloned.1.call-start = ((), (), s32[]{:S(2)}) async-start(), calls=%async_computation.3 | async-start | bytes 589824 | tf_op jit(solution)/shard_map/reduce_scatter | solution.py:107
  8.4 4.8 %copy-start.11 = (bf16[2048,4]{0,1:T(4,128)(2,1)S(1)}, bf16[2048,4]{0,1:T(4,128)(2,1)}, u32[]{:S(2)}) copy-start(bf16[2048,4]{0,1:T(4,128)(2,1)} %param.26) | copy-start | bytes 49156
  13.6 8.2 %copy-start.1 = (f32[24,4,128,128]{3,2,1,0:T(8,128)S(1)}, f32[24,4,128,128]{3,2,1,0:T(8,128)}, u32[]{:S(2)}) copy-start(f32[24,4,128,128]{3,2,1,0:T(8,128)} %param.29) | copy-start | bytes 18874372
  21.8 3.9 %copy-start.3 = (bf16[2048,512]{1,0:T(8,128)(2,1)S(1)}, bf16[2048,512]{1,0:T(8,128)(2,1)}, u32[]{:S(2)}) copy-start(bf16[2048,512]{1,0:T(8,128)(2,1)} %param.21) | copy-start | bytes 6291460
  26.4 7.7 %copy-start.4 = (bf16[2048,512]{1,0:T(8,128)(2,1)S(1)}, bf16[2048,512]{1,0:T(8,128)(2,1)}, u32[]{:S(2)}) copy-start(bf16[2048,512]{1,0:T(8,128)(2,1)} %param.24) | copy-start | bytes 6291460
  33.9 0.7 copy-start.9
  34.5 2.9 %copy-start.7 = (f32[2048]{0:T(1024)S(1)}, f32[2048]{0:T(1024)}, u32[]{:S(2)}) copy-start(f32[2048]{0:T(1024)} %param.32) | copy-start | bytes 24580
  34.5 3.1 %copy-start.6 = (s32[24,2]{0,1:T(2,128)S(1)}, s32[24,2]{0,1:T(2,128)}, u32[]{:S(2)}) copy-start(s32[24,2]{0,1:T(2,128)} %param.36) | copy-start | bytes 580
  62.1 27.2 %copy-start.8 = (f32[24,2]{0,1:T(2,128)S(1)}, f32[24,2]{0,1:T(2,128)}, u32[]{:S(2)}) copy-start(f32[24,2]{0,1:T(2,128)} %param.37) | copy-start | bytes 580
  72.1 17.1 %all-to-all-start.1 = ((bf16[1,16,6,1024]{3,2,0,1:T(8,128)(2,1)}), bf16[1,16,6,1024]{3,2,0,1:T(8,128)(2,1)S(1)}, u32[]{:S(2)}, u32[]{:S(2)}) async-start(bf16[1,16,6,1024]{3,2,0,1:T(8,128)(2,1)} %copy.55), calls=%async_computation.2 | async-start | bytes 524288 | tf_op jit(solution)/shard_map/all_to_all | solution.py:108
Sparse Core Ops, SparseCore 0:
  64.6 5.7 reduce-scatter.1
